TPU v7x, 256 devices: a whole 4x4x8 slice. The times are simulated.
256 devices in a mesh: ep: 64 (over z, y, core), tp: 4 (over x).
Axes of the slice: x: 4, y: 4, z: 8, core: 2. Of those that a mesh axis runs over, the one named last changes fastest.
Arguments:
- mixer_input: bfloat16 [32768, 2048], P(('ep', 'tp')), may hold values from -6 to 6
- expert_input: bfloat16 [32768, 2048], P(('ep', 'tp')), may hold values from -6 to 6
- mixer_gain: float32 [2048], replicated, may hold values from 0.1 to 1.9
- expert_gain: float32 [2048], replicated, may hold values from 0.1 to 1.9
- query_weight: bfloat16 [2048, 1024], P(None, 'tp'), may hold values from -0.125 to 0.125
- key_weight: bfloat16 [2048, 1024], P(None, 'tp'), may hold values from -0.125 to 0.125
- value_weight: bfloat16 [2048, 1024], P(None, 'tp'), may hold values from -0.125 to 0.125
- out_weight: bfloat16 [1024, 2048], P('tp'), may hold values from -0.1875 to 0.1875
- decay_rate: float32 [8], P('tp'), may hold values from 0 to 0.12
- routing: int32 [32768, 4], P('ep'), may hold values from 0 to 63, all different within a row; in each aligned block of 128 rows (0 to 127, 128 to 255, ...) at most 12 rows name the same one
- route_weight: float32 [32768, 4], P('ep'), may hold values from 0.2 to 1
- gate_weight: bfloat16 [64, 2048, 1024], P('ep', None, 'tp'), may hold values from -0.125 to 0.125
- up_weight: bfloat16 [64, 2048, 1024], P('ep', None, 'tp'), may hold values from -0.125 to 0.125
- down_weight: bfloat16 [64, 1024, 2048], P('ep', None, 'tp'), may hold values from -0.1875 to 0.1875
- shared_gate: bfloat16 [2048, 512], P(None, 'tp'), may hold values from -0.125 to 0.125
- shared_up: bfloat16 [2048, 512], P(None, 'tp'), may hold values from -0.125 to 0.125
- shared_down: bfloat16 [512, 2048], P(None, 'tp'), may hold values from -0.25 to 0.25
Outputs:
- mixer_output: float32 [32768, 2048], P(('ep', 'tp'))
- expert_output: float32 [32768, 2048], P('ep', 'tp')
Inputs may be any that keep to these rules, and one draw needn't show every extreme that they name: `routing`: each row names 4 different experts. In each aligned block of 128 rows, no expert is named by more than 12 rows, and in some blocks one expert is named by exactly 12 rows.
All inputs are finite; a program needn't handle non-finite values.
Results may differ from a plain program's by a relative error of at most 0.0095.
Values may be sent and summed in bfloat16 or wider, within the bound.
A program may use at most 128 MiB of HBM per device.

v0:
```python
import jax
import jax.numpy as jnp
from jax import lax
from jax.sharding import Mesh
from jax.sharding import PartitionSpec as P

HD = 128
BLK = 64
EP = ("ep_0", "ep_1", "ep_2")
EP_TP = ("ep_0", "ep_1", "ep_2", "tp")
NORM_EPS = 1e-06
ROPE_BASE = 10000.0
EXACT_MATMUL = lax.Precision.HIGHEST


def nothing_yet(value, identity):
    return jax.tree.map(
        lambda a, e: jnp.broadcast_to(jnp.asarray(e, a.dtype), a.shape), value, identity
    )


def entering_2(value, axes, combine, identity):
    before = start = nothing_yet(value, identity)
    subtotal = value
    for axis in reversed(axes):
        count, mine = (lax.axis_size(axis), lax.axis_index(axis))
        pieces = jax.tree.map(lambda part: lax.all_gather(part, axis), subtotal)
        inside, subtotal = (start, start)
        for k in range(count):
            passed = k < mine
            subtotal = combine(subtotal, jax.tree.map(lambda part: part[k], pieces))
            inside = jax.tree.map(lambda new, old: jnp.where(passed, new, old), subtotal, inside)
        before = combine(inside, before)
    return before


def sent_together(arrays, axis, dim, along):
    ends, at = ([], 0)
    for a in arrays[:-1]:
        at += a.shape[along]
        ends.append(at)
    both = jnp.concatenate(arrays, axis=along)
    return tuple(jnp.split(lax.all_gather(both, axis, axis=dim, tiled=True), ends, axis=along))


def norm_rows(inputs, gain_vector):
    values = inputs.astype(jnp.float32)
    scaled = values * lax.rsqrt(jnp.mean(values * values, axis=-1, keepdims=True) + NORM_EPS)
    return (scaled * gain_vector).astype(jnp.bfloat16)


def rotate(head_rows, positions):
    head_size = head_rows.shape[-1]
    inverse = ROPE_BASE ** (-jnp.arange(0, head_size, 2, dtype=jnp.float32) / head_size)
    angles = positions[:, None] * inverse[None, :]
    cosine = jnp.cos(angles)[:, None, :]
    sine_part = jnp.sin(angles)[:, None, :]
    front_half = head_rows[..., : head_size // 2]
    behind = head_rows[..., head_size // 2 :]
    return jnp.concatenate(
        [front_half * cosine - behind * sine_part, front_half * sine_part + behind * cosine],
        axis=-1,
    )


def project(inputs, weight, head_total):
    product = jnp.dot(inputs, weight, preferred_element_type=jnp.float32).astype(jnp.bfloat16)
    product = lax.optimization_barrier(product)
    return product.astype(jnp.float32).reshape(inputs.shape[0], head_total, -1)


def chain_combine(earlier, latter):
    return (earlier[0] * latter[0], latter[0][:, None, None] * earlier[1] + latter[1])


def retain_local(query_heads, key_heads, value_heads, decay_rates):
    length, head_total, head_size = query_heads.shape
    blocks = length // BLK
    log_gamma = -decay_rates
    inner_pos = jnp.arange(BLK, dtype=jnp.float32)
    offsets = inner_pos[:, None] - inner_pos[None, :]
    inside_block_output = jnp.where(
        offsets >= 0, jnp.exp(log_gamma[:, None, None] * jnp.maximum(offsets, 0.0)), 0.0
    )
    key_scale = jnp.exp(log_gamma[None, :] * (BLK - 1.0 - inner_pos)[:, None])
    query_scale = jnp.exp(log_gamma[None, :] * (inner_pos + 1.0)[:, None])
    blocked = (blocks, BLK, head_total, head_size)
    q_blocks = query_heads.reshape(blocked)
    k_blocks = key_heads.reshape(blocked)
    v_blocks = value_heads.reshape(blocked)
    attention_scores = (
        jnp.einsum("nchd,nmhd->nhcm", q_blocks, k_blocks, precision=EXACT_MATMUL)
        * inside_block_output[None]
    )
    nearby = jnp.einsum("nhcm,nmhe->nche", attention_scores, v_blocks, precision=EXACT_MATMUL)
    block_states = jnp.einsum(
        "nchd,nche->nhde", k_blocks * key_scale[None, :, :, None], v_blocks, precision=EXACT_MATMUL
    )
    block_offset_rows = jnp.arange(blocks, dtype=jnp.float32)
    to_end = jnp.exp(log_gamma[None, :] * BLK * (blocks - 1.0 - block_offset_rows)[:, None])
    summary = jnp.einsum("nh,nhde->hde", to_end, block_states, precision=EXACT_MATMUL)
    through = jnp.exp(log_gamma * (BLK * blocks))
    incoming = entering_2(
        (through, summary), EP, chain_combine, (jnp.ones_like(through), jnp.zeros_like(summary))
    )[1]
    block_gaps = block_offset_rows[:, None] - 1.0 - block_offset_rows[None, :]
    carry_mix = jnp.where(
        block_gaps >= 0, jnp.exp(log_gamma[:, None, None] * BLK * jnp.maximum(block_gaps, 0.0)), 0.0
    )
    entering = jnp.einsum("hbj,jhde->bhde", carry_mix, block_states, precision=EXACT_MATMUL)
    entering = (
        entering
        + jnp.exp(log_gamma[None, :] * BLK * block_offset_rows[:, None])[:, :, None, None]
        * incoming[None]
    )
    distant = jnp.einsum(
        "bchd,bhde->bche",
        q_blocks * query_scale[None, :, :, None],
        entering,
        precision=EXACT_MATMUL,
    )
    retained = (nearby + distant).reshape(length, head_total, head_size)
    normed = retained * lax.rsqrt(jnp.mean(retained * retained, axis=-1, keepdims=True) + NORM_EPS)
    return normed.astype(jnp.bfloat16).reshape(length, head_total * head_size)


def assign_slots(routes, source_rows, capacity, expert_count):
    token_count, pick_count = routes.shape
    chosen = routes.reshape(token_count * pick_count)
    onehot = (chosen[:, None] == jnp.arange(expert_count, dtype=jnp.int32)[None, :]).astype(
        jnp.int32
    )
    per_source = onehot.reshape(token_count // source_rows, source_rows * pick_count, expert_count)
    earlier_hits = jnp.cumsum(per_source, axis=1) - per_source
    ranks = jnp.sum(earlier_hits * per_source, axis=2).reshape(token_count * pick_count)
    sources = jnp.arange(token_count * pick_count, dtype=jnp.int32) // (source_rows * pick_count)
    return (chosen, sources * capacity + ranks)


def gather_slots(token_rows, chosen, slot_ids, slot_count, expert_count, pick_count):
    owners = jnp.arange(chosen.shape[0], dtype=jnp.int32) // pick_count + 1
    owner_table = jnp.zeros((slot_count, expert_count), jnp.int32).at[slot_ids, chosen].set(owners)
    padded = jnp.concatenate(
        [jnp.zeros((1, token_rows.shape[1]), token_rows.dtype), token_rows], axis=0
    )
    return padded[owner_table]


def expert_hidden(routed_rows, gate_weight, up_weight):
    per_device = gate_weight.shape[0]
    grouped = routed_rows.reshape(
        routed_rows.shape[0], routed_rows.shape[1] // per_device, per_device, routed_rows.shape[2]
    )
    gate_part = jnp.einsum(
        "snxd,xdf->snxf", grouped, gate_weight, preferred_element_type=jnp.float32
    )
    up_part = jnp.einsum("snxd,xdf->snxf", grouped, up_weight, preferred_element_type=jnp.float32)
    return (jax.nn.silu(gate_part) * up_part).astype(jnp.bfloat16)


def shards(
    mixer_input,
    expert_input,
    mixer_gain,
    expert_gain,
    query_weight,
    key_weight,
    value_weight,
    out_weight,
    decay_rate,
    routing,
    route_weight,
    gate_weight,
    up_weight,
    down_weight,
    shared_gate,
    shared_up,
    shared_down,
):
    own_count = mixer_input.shape[0]
    tp_index = lax.axis_index("tp")
    own_expert_rows = norm_rows(expert_input, expert_gain)
    mixer_rows, expert_rows = sent_together(
        (norm_rows(mixer_input, mixer_gain), own_expert_rows), "tp", 0, 1
    )
    group_count = mixer_rows.shape[0]
    head_total = decay_rate.shape[0]
    positions = (
        lax.axis_index(EP) * group_count + jnp.arange(group_count, dtype=jnp.int32)
    ).astype(jnp.float32)
    query_heads = rotate(project(mixer_rows, query_weight, head_total), positions) * HD ** (-0.5)
    key_heads = rotate(project(mixer_rows, key_weight, head_total), positions)
    value_heads = project(mixer_rows, value_weight, head_total)
    mixed_heads = retain_local(query_heads, key_heads, value_heads, decay_rate)
    mixer_output = lax.psum_scatter(
        jnp.dot(mixed_heads, out_weight, preferred_element_type=jnp.float32).astype(jnp.bfloat16),
        "tp",
        scatter_dimension=0,
        tiled=True,
    ).astype(jnp.float32)
    expert_count = lax.axis_size(EP) * gate_weight.shape[0]
    pick_count = routing.shape[1]
    capacity = (3 * own_count * pick_count + 2 * expert_count - 1) // (2 * expert_count)
    chosen, slot_ids = assign_slots(routing, own_count, capacity, expert_count)
    own_span = own_count * pick_count
    own_chosen = lax.dynamic_slice_in_dim(chosen, tp_index * own_span, own_span, 0)
    own_slots = (
        lax.dynamic_slice_in_dim(slot_ids, tp_index * own_span, own_span, 0) - tp_index * capacity
    )
    outgoing = gather_slots(
        own_expert_rows, own_chosen, own_slots, capacity, expert_count, pick_count
    )
    arrived = lax.all_to_all(outgoing, EP, split_axis=1, concat_axis=1, tiled=True)
    hidden = expert_hidden(
        lax.all_gather(arrived, "tp", axis=0, tiled=True), gate_weight, up_weight
    )
    shared_hidden = (
        jax.nn.silu(jnp.dot(expert_rows, shared_gate, preferred_element_type=jnp.float32))
        * jnp.dot(expert_rows, shared_up, preferred_element_type=jnp.float32)
    ).astype(jnp.bfloat16)
    full_hidden, full_shared = (
        lax.all_gather(hidden, "tp", axis=3, tiled=True),
        lax.all_gather(shared_hidden, "tp", axis=1, tiled=True),
    )
    results = jnp.einsum(
        "snxf,xfe->snxe", full_hidden, down_weight, preferred_element_type=jnp.float32
    ).astype(jnp.bfloat16)
    results = results.reshape(results.shape[0], expert_count, results.shape[3])
    returned = lax.all_to_all(results, EP, split_axis=1, concat_axis=1, tiled=True)
    flat_results = returned.reshape(returned.shape[0] * expert_count, returned.shape[2])
    picked = flat_results[slot_ids * expert_count + chosen].astype(jnp.float32)
    weighted = jnp.sum(
        picked.reshape(group_count, pick_count, -1) * route_weight[:, :, None], axis=1
    )
    shared_result = jnp.dot(full_shared, shared_down, preferred_element_type=jnp.float32)
    expert_output = weighted + shared_result
    return (mixer_output, expert_output)


def solution(mesh):
    finer = Mesh(mesh.devices.reshape(8, 4, 2, mesh.shape["tp"]), ("ep_0", "ep_1", "ep_2", "tp"))
    placed = (
        P(EP_TP, None),
        P(EP_TP, None),
        P(),
        P(),
        P(None, "tp"),
        P(None, "tp"),
        P(None, "tp"),
        P("tp", None),
        P("tp"),
        P(EP, None),
        P(EP, None),
        P(EP, None, "tp"),
        P(EP, None, "tp"),
        P(EP, None, "tp"),
        P(None, "tp"),
        P(None, "tp"),
        P(None, "tp"),
    )
    return jax.shard_map(
        shards,
        mesh=finer,
        in_specs=placed,
        out_specs=(P(EP_TP, None), P(EP, "tp")),
        check_vma=False,
    )
```

profile of v0, /device:TPU:8, one launch (start us, length us, event | category | flops | bytes accessed | tf_op | source)
XLA Modules:
  0.0 539.4 jit_solution(6858122981832166352)
XLA Ops:
  11.3 4.8 reduce-window.6
  17.0 25.4 %scatter_fusion = s32[12,64]{1,0:T(8,128)S(1)} fusion(s32[12,64]{1,0:T(8,128)S(1)} %broadcast.456, s32[512]{0:T(512)S(1)} %bitcast.156, s32[512]{0:T(512)S(1)} %fusion.96), kind=kCustom, calls=%fused_computation.2 | custom fusion | bytes 10240 | tf_op jit(solution)/shard_map/scatter | solution.py:142
  43.6 4.3 gather_fusion
  47.9 3.7 copy.112
  51.5 108.1 %all_to_all.10 = bf16[12,64,2048]{2,0,1:T(8,128)(2,1)S(1)} all-to-all(bf16[12,64,2048]{2,0,1:T(8,128)(2,1)S(1)} %copy.112), channel_id=1, replica_groups=mesh['ep_0'=8,'ep_1'=4,'ep_2'=2,'tp'=4] {'ep_0','ep_1','ep_2'}, dimensions={1} | all-to-all | bytes 6291456 | tf_op jit(solution)/shard_map/all_to_all | solution.py:213
  159.6 3.4 copy.113
  165.6 114.8 %all-gather.13.cloned.1.call-done = bf16[48,64,2048]{2,1,0:T(8,128)(2,1)} async-done(((bf16[12,64,2048]{2,1,0:T(8,128)(2,1)}), bf16[48,64,2048]{2,1,0:T(8,128)(2,1)}) %all-gather.13.cloned.1.call-update) | async-done | bytes 12582928 | tf_op jit(solution)/shard_map/all_gather | solution.py:215
  280.4 7.9 %fusion.43 = f32[48,64,256]{2,1,0:T(8,128)S(1)} fusion(bf16[48,64,2048]{2,1,0:T(8,128)(2,1)} %all-gather.13.cloned.1.call-done, bf16[1,2048,256]{2,1,0:T(8,128)(2,1)} %param.29), kind=kOutput, calls=%fused_computation.48 | convolution fusion | flops 3221225472 | bytes 16777216 | tf_op jit(solution)/shard_map/snxd,xdf->snxf/dot_general | solution.py:157
  288.9 5.2 fusion.2
  299.4 8.6 %all-reduce.2 = f32[8]{0:T(128)S(1)} all-reduce(f32[8]{0:T(128)S(1)} %get-tuple-element.36), channel_id=4, replica_groups=mesh['ep_0'=8,'ep_1'=4,'ep_2'=2,'tp'=4] {'ep_1'}, use_global_device_ids=true, to_apply=%add.2 | all-reduce | flops 8 | bytes 64
  308.7 16.6 %all-gather.3 = f32[8,1,2]{2,1,0:T(1,128)S(1)} all-gather(f32[1,1,2]{2,1,0:T(1,128)S(1)} %get-tuple-element.28), channel_id=1, replica_groups=mesh['ep_0'=8,'ep_1'=4,'ep_2'=2,'tp'=4] {'ep_0'}, dimensions={0}, use_global_device_ids=true | all-gather | bytes 72 | tf_op jit(solution)/shard_map/all_gather | solution.py:27
  329.1 5.5 %all-gather.9.cloned.1.call-done = bf16[512,4096]{1,0:T(8,128)(2,1)} async-done(((bf16[128,4096]{1,0:T(8,128)(2,1)}), bf16[512,4096]{1,0:T(8,128)(2,1)}) %all-gather.9.cloned.1.call-update) | async-done | bytes 4194320 | tf_op jit(solution)/shard_map/all_gather | solution.py:43
  351.2 12.8 %all_gather.47 = f32[4,2,128,128]{3,2,1,0:T(8,128)S(1)} all-gather(f32[1,2,128,128]{3,2,1,0:T(8,128)S(1)} %fusion.72), channel_id=1, replica_groups=mesh['ep_0'=8,'ep_1'=4,'ep_2'=2,'tp'=4] {'ep_1'}, dimensions={0}, use_global_device_ids=true | all-gather | bytes 655360 | tf_op jit(solution)/shard_map/all_gather | solution.py:27
  364.9 43.6 %all-gather.15.cloned.1.call-done = bf16[48,64,1,1024]{3,1,0,2:T(8,128)(2,1)} async-done(((bf16[48,64,1,256]{3,1,0,2:T(8,128)(2,1)}), bf16[48,64,1,1024]{3,1,0,2:T(8,128)(2,1)}) %all-gather.15.cloned.1.call-update) | async-done | bytes 6291472 | tf_op jit(solution)/shard_map/all_gather | solution.py:222
  408.5 6.4 %fusion.6 = bf16[48,64,512]{2,1,0:T(8,128)(2,1)S(1)} fusion(bf16[48,64,1,1024]{3,1,0,2:T(8,128)(2,1)} %all-gather.15.cloned.1.call-done, bf16[1,1024,512]{2,1,0:T(8,128)(2,1)S(1)} %copy-done), kind=kOutput, calls=%fused_computation.14 | convolution fusion | flops 3222798336 | bytes 10485760 | tf_op jit(solution)/shard_map/snxf,xfe->snxe/dot_general | solution.py:225
  414.9 3.4 copy.114
  418.3 10.9 %all-to-all-start.1 = ((bf16[48,64,512]{2,0,1:T(8,128)(2,1)}), bf16[48,64,512]{2,0,1:T(8,128)(2,1)}, u32[]{:S(2)}, u32[]{:S(2)}) async-start(bf16[48,64,512]{2,0,1:T(8,128)(2,1)} %copy.114), calls=%async_computation.2 | async-start | bytes 6291456 | tf_op jit(solution)/shard_map/all_to_all | solution.py:229
  434.5 24.3 %all-gather.11.cloned.1.call-done = f32[8,2,128,128]{3,2,1,0:T(8,128)} async-done(((f32[1,2,128,128]{3,2,1,0:T(8,128)}), f32[8,2,128,128]{3,2,1,0:T(8,128)}) %all-gather.11.cloned.1.call-update) | async-done | bytes 1048592 | tf_op jit(solution)/shard_map/all_gather | solution.py:27
  465.0 3.4 convolution_convert_fusion
  473.4 18.1 %all_gather.51 = bf16[512,512]{1,0:T(8,128)(2,1)} all-gather(bf16[512,128]{1,0:T(8,128)(2,1)S(1)} %fusion.33), channel_id=1, replica_groups=mesh['ep_0'=8,'ep_1'=4,'ep_2'=2,'tp'=4] {'tp'}, dimensions={1}, use_global_device_ids=true | all-gather | bytes 655360 | tf_op jit(solution)/shard_map/all_gather | solution.py:223
  491.5 12.0 %reduce-scatter.2.cloned.1.call-done = bf16[128,2048]{1,0:T(8,128)(2,1)} async-done(((bf16[512,2048]{1,0:T(8,128)(2,1)}), bf16[128,2048]{1,0:T(8,128)(2,1)}) %reduce-scatter.2.cloned.1.call-update) | async-done | bytes 524304 | tf_op jit(solution)/shard_map/reduce_scatter | solution.py:195
  508.1 5.3 copy.115
  513.4 9.9 %gather_fusion.1 = bf16[2048,512]{1,0:T(8,128)(2,1)S(1)} fusion(bf16[3072,512]{1,0:T(8,128)(2,1)} %bitcast.155, s32[2048]{0:T(1024)S(1)} %broadcast_clamp_fusion), kind=kCustom, calls=%fused_computation.1 | custom fusion | bytes 4202496 | tf_op jit(solution)/shard_map/gather | solution.py:231
  526.3 4.9 multiply_reduce_fusion
  (166 shorter events, 60.2 us)
Async XLA Ops:
  7.2 401.3 %copy-start = (bf16[1,1024,512]{2,1,0:T(8,128)(2,1)S(1)}, bf16[1,1024,512]{2,1,0:T(8,128)(2,1)}, u32[]{:S(2)}) copy-start(bf16[1,1024,512]{2,1,0:T(8,128)(2,1)} %param.30) | copy-start | bytes 3145732
  7.2 273.3 %all-gather.13.cloned.1.call-start = ((), (), s32[]{:S(2)}) async-start(), calls=%async_computation.6 | async-start | bytes 15728640 | tf_op jit(solution)/shard_map/all_gather | solution.py:215
  11.2 31.2 %copy-start.6 = (bf16[128,2048]{1,0:T(8,128)(2,1)S(1)}, bf16[128,2048]{1,0:T(8,128)(2,1)}, u32[]{:S(2)}) copy-start(bf16[128,2048]{1,0:T(8,128)(2,1)} %param.17) | copy-start | bytes 1572868
  11.2 31.2 %copy-start.12 = (f32[2048]{0:T(1024)S(1)}, f32[2048]{0:T(1024)}, u32[]{:S(2)}) copy-start(f32[2048]{0:T(1024)} %param.19) | copy-start | bytes 24580
  11.2 31.2 %copy-start.13 = (f32[2048]{0:T(1024)S(1)}, f32[2048]{0:T(1024)}, u32[]{:S(2)}) copy-start(f32[2048]{0:T(1024)} %param.20) | copy-start | bytes 24580
  163.0 171.6 %all-gather.9.cloned.1.call-start = ((), (), s32[]{:S(2)}) async-start(), calls=%async_computation.3 | async-start | bytes 5242880 | tf_op jit(solution)/shard_map/all_gather | solution.py:43
  165.1 123.3 %copy-start.32 = (bf16[1,2048,256]{2,1,0:T(8,128)(2,1)S(1)}, bf16[1,2048,256]{2,1,0:T(8,128)(2,1)}, u32[]{:S(2)}) copy-start(bf16[1,2048,256]{2,1,0:T(8,128)(2,1)} %param.28) | copy-start | bytes 3145732
  165.1 243.4 %all-gather.15.cloned.1.call-start = ((), (), s32[]{:S(2)}) async-start(), calls=%async_computation.7 | async-start | bytes 7864320 | tf_op jit(solution)/shard_map/all_gather | solution.py:222
  294.1 164.7 %all-gather.11.cloned.1.call-start = ((), (), s32[]{:S(2)}) async-start(), calls=%async_computation.4 | async-start | bytes 1179648 | tf_op jit(solution)/shard_map/all_gather | solution.py:27
  295.5 41.7 %copy-start.15 = (f32[2]{0:T(128)}, f32[2]{0:T(128)S(1)}, u32[]{:S(2)}) copy-start(f32[2]{0:T(128)S(1)} %get-tuple-element.39) | copy-start | bytes 28
  418.3 89.7 %all-to-all-start.1 = ((bf16[48,64,512]{2,0,1:T(8,128)(2,1)}), bf16[48,64,512]{2,0,1:T(8,128)(2,1)}, u32[]{:S(2)}, u32[]{:S(2)}) async-start(bf16[48,64,512]{2,0,1:T(8,128)(2,1)} %copy.114), calls=%async_computation.2 | async-start | bytes 6291456 | tf_op jit(solution)/shard_map/all_to_all | solution.py:229
  429.2 29.6 %copy-start.19 = (f32[2]{0:T(128)S(1)}, f32[2]{0:T(128)}, u32[]{:S(2)}) copy-start(f32[2]{0:T(128)} %get-tuple-element.31) | copy-start | bytes 28
  429.2 29.6 %copy-start.20 = (f32[2]{0:T(128)S(1)}, f32[2]{0:T(128)}, u32[]{:S(2)}) copy-start(f32[2]{0:T(128)} %get-tuple-element.32) | copy-start | bytes 28
  429.2 29.6 %copy-start.21 = (f32[2]{0:T(128)S(1)}, f32[2]{0:T(128)}, u32[]{:S(2)}) copy-start(f32[2]{0:T(128)} %get-tuple-element.14) | copy-start | bytes 28
  429.2 29.6 %copy-start.22 = (f32[2]{0:T(128)S(1)}, f32[2]{0:T(128)}, u32[]{:S(2)}) copy-start(f32[2]{0:T(128)} %get-tuple-element.15) | copy-start | bytes 28
  429.2 29.6 %copy-start.23 = (f32[2]{0:T(128)S(1)}, f32[2]{0:T(128)}, u32[]{:S(2)}) copy-start(f32[2]{0:T(128)} %get-tuple-element.16) | copy-start | bytes 28
  429.3 29.6 %copy-start.24 = (f32[2]{0:T(128)S(1)}, f32[2]{0:T(128)}, u32[]{:S(2)}) copy-start(f32[2]{0:T(128)} %get-tuple-element.17) | copy-start | bytes 28
  429.3 29.6 %copy-start.25 = (f32[2]{0:T(128)S(1)}, f32[2]{0:T(128)}, u32[]{:S(2)}) copy-start(f32[2]{0:T(128)} %get-tuple-element.18) | copy-start | bytes 28
  429.3 29.6 %copy-start.26 = (f32[2]{0:T(128)S(1)}, f32[2]{0:T(128)}, u32[]{:S(2)}) copy-start(f32[2]{0:T(128)} %get-tuple-element.19) | copy-start | bytes 28
  429.3 31.4 %copy-start.16 = (f32[2]{0:T(128)S(1)}, f32[2]{0:T(128)}, u32[]{:S(2)}) copy-start(f32[2]{0:T(128)} %copy-done.15) | copy-start | bytes 28
  429.3 31.4 %copy-start.18 = (f32[8,2]{0,1:T(2,128)S(1)}, f32[8,2]{0,1:T(2,128)}, u32[]{:S(2)}) copy-start(f32[8,2]{0,1:T(2,128)} %get-tuple-element.26) | copy-start | bytes 196
  429.3 74.2 %reduce-scatter.2.cloned.1.call-start = ((), (), s32[]{:S(2)}) async-start(), calls=%async_computation.5 | async-start | bytes 2621440 | tf_op jit(solution)/shard_map/reduce_scatter | solution.py:195
  432.3 30.1 %copy-start.1 = (f32[512,2,64]{2,0,1:T(8,128)S(1)}, f32[512,2,64]{2,0,1:T(8,128)}, u32[]{:S(2)}) copy-start(f32[512,2,64]{2,0,1:T(8,128)} %get-tuple-element.4) | copy-start | bytes 786436
  432.3 30.1 %copy-start.17 = (f32[64,2]{0,1:T(2,128)S(1)}, f32[64,2]{0,1:T(2,128)}, u32[]{:S(2)}) copy-start(f32[64,2]{0,1:T(2,128)} %get-tuple-element.24) | copy-start | bytes 1540
  (19 other events, 139.9 us)
Sparse Core Ops, SparseCore 0:
  163.1 117.2 all-gather.12
  282.8 51.7 all-gather.8
  336.4 72.0 all-gather.14
  410.1 48.6 all-gather.10
  468.5 34.9 reduce-scatter.1
where the time goes:
time: 547 us; the launch traced here: 539 us
  waiting for transfers between devices  203 us (37%)
  blocking collectives  169 us (31%)
  local copies, waits for them, and re-layouts  67.4 us (12%)
  matrix products  46.5 us (9%)
  other arithmetic  26.2 us (5%)
  between operations  16.1 us (3%)
  starting transfers between devices  11.5 us (2%)
    all_gather x1, waiting for transfers between devices, shards(): lax.all_gather(arrived, 'tp', axis=0, tiled=True)  115 us
    all_to_all x1, blocking collectives, shards(): lax.all_to_all(outgoing, EP, split_axis=1, concat_axis=1, tiled=True)  108 us
    all_gather x1, waiting for transfers between devices, shards(): lax.all_gather(hidden, 'tp', axis=3, tiled=True)  43.6 us
    all_gather x3, blocking collectives, entering_2(): pieces = jax.tree.map(lambda part: lax.all_gather(part, axis), subtotal)  31.6 us
    scatter x1, local copies, waits for them, and re-layouts, gather_slots(): jnp.zeros((slot_count, expert_count), jnp.int32).at[slot_ids, chosen]  25.4 us
    all_gather x1, waiting for transfers between devices, entering_2(): pieces = jax.tree.map(lambda part: lax.all_gather(part, axis), subtotal)  24.3 us
    all_gather x1, blocking collectives, shards(): lax.all_gather(shared_hidden, 'tp', axis=1, tiled=True)  18.1 us
    reduce_scatter x1, waiting for transfers between devices, shards(): lax.psum_scatter(jnp.dot(mixed_heads, out_weight, preferred_element_type=...  12 us
  transfers between devices with their start and end apart: 6, of which 6 were waited for; matrix products, arithmetic and copies ran while one was open for 12% of the time, Pallas kernels for 0%

commit v1 on v0

--- a/solution.py
+++ b/solution.py
@@ -3,6 +3,7 @@
 from jax import lax
 from jax.sharding import Mesh
 from jax.sharding import PartitionSpec as P
+from jax.lax import axis_index, ppermute, psum
 
 HD = 128
 BLK = 64
@@ -11,6 +12,35 @@
 NORM_EPS = 1e-06
 ROPE_BASE = 10000.0
 EXACT_MATMUL = lax.Precision.HIGHEST
+
+
+def cut_goods_on(base_x):
+    small = psum(1, axis_name="tp")
+    base_arr, b_now, after = (small, axis_index("tp"), base_x.shape[3])
+    response = jnp.zeros(
+        [k0 * base_arr if kk == 3 else k0 for kk, k0 in enumerate(base_x.shape)], base_x.dtype
+    )
+    prior = lax.dynamic_update_slice_in_dim(response, base_x, b_now * after, axis=3)
+    carry_out = n_now = base_x
+    for i in range(1, base_arr // 2 + 1):
+        carry_out = ppermute(
+            carry_out,
+            axis_name="tp",
+            perm=list(map(lambda kk: (kk, (kk + 1) % base_arr), range(base_arr))),
+        )
+        prior = lax.dynamic_update_slice_in_dim(
+            prior, carry_out, (b_now - i) % base_arr * after, axis=3
+        )
+        if 2 * i < base_arr:
+            n_now = ppermute(
+                n_now,
+                axis_name="tp",
+                perm=list(map(lambda kk: (kk, (kk - 1) % base_arr), range(base_arr))),
+            )
+            prior = lax.dynamic_update_slice_in_dim(
+                prior, n_now, (b_now + i) % base_arr * after, axis=3
+            )
+    return prior
 
 
 def nothing_yet(value, identity):
@@ -219,7 +249,7 @@
         * jnp.dot(expert_rows, shared_up, preferred_element_type=jnp.float32)
     ).astype(jnp.bfloat16)
     full_hidden, full_shared = (
-        lax.all_gather(hidden, "tp", axis=3, tiled=True),
+        cut_goods_on(hidden),
         lax.all_gather(shared_hidden, "tp", axis=1, tiled=True),
     )
     results = jnp.einsum(

time: 547 us -> 508 us (0.929)
  waiting for transfers between devices: 203 us -> 157 us
  local copies, waits for them, and re-layouts: 67.4 us -> 77.3 us
    all_gather x1 -> x0, waiting for transfers between devices: 43.6 us -> none  [shards(): lax.all_gather(hidden, 'tp', axis=3, tiled=True)]
    ppermute x0 -> x3, waiting for transfers between devices: none -> 43.1 us  [the longest x2 43.1 us: cut_goods_on(): ppermute(carry_out, axis_name='tp', perm=list(map(lambda kk: (kk, (kk + 1...]
    all_gather x1, waiting for transfers between devices: 115 us -> 80.1 us  [shards(): lax.all_gather(arrived, 'tp', axis=0, tiled=True)]
    all_gather x1, waiting for transfers between devices: 24.3 us -> 0.02 us  [entering_2(): pieces = jax.tree.map(lambda part: lax.all_gather(part, axis), subtotal)]
    all_to_all x1, waiting for transfers between devices: 2.43 us -> 21.8 us  [shards(): lax.all_to_all(results, EP, split_axis=1, concat_axis=1, tiled=True)]
    dynamic_update_slice x0 -> x3, local copies, waits for them, and re-layouts: none -> 8.55 us  [the longest x2 5.69 us: cut_goods_on(): lax.dynamic_update_slice_in_dim(prior, carry_out, (b_now - i) % base_arr...]
    all_gather x1, waiting for transfers between devices: 5.5 us -> 0.01 us  [sent_together(): lax.all_gather(both, axis, axis=dim, tiled=True)]
  transfers between devices with their start and end apart: 6 -> 8, of which waited for: 6 -> 5; matrix products, arithmetic and copies ran while one was open for 12% -> 19% of each run, Pallas kernels for 0% -> 0%
where the time goes in v1:
time: 508 us; the launch traced here: 500 us
  blocking collectives  168 us (33%)
  waiting for transfers between devices  157 us (31%)
  local copies, waits for them, and re-layouts  77.3 us (15%)
  matrix products  42.6 us (8%)
  other arithmetic  24.8 us (5%)
  between operations  16 us (3%)
  starting transfers between devices  14.9 us (3%)
    all_to_all x1, blocking collectives, shards(): lax.all_to_all(outgoing, EP, split_axis=1, concat_axis=1, tiled=True)  108 us
    all_gather x1, waiting for transfers between devices, shards(): lax.all_gather(arrived, 'tp', axis=0, tiled=True)  80.1 us
    ppermute x2, waiting for transfers between devices, cut_goods_on(): ppermute(carry_out, axis_name='tp', perm=list(map(lambda kk: (kk, (kk + 1...  43.1 us
    all_gather x3, blocking collectives, entering_2(): pieces = jax.tree.map(lambda part: lax.all_gather(part, axis), subtotal)  29.2 us
    scatter x1, local copies, waits for them, and re-layouts, gather_slots(): jnp.zeros((slot_count, expert_count), jnp.int32).at[slot_ids, chosen]  25.4 us
    all_to_all x1, waiting for transfers between devices, shards(): lax.all_to_all(results, EP, split_axis=1, concat_axis=1, tiled=True)  21.8 us
    all_gather x1, blocking collectives, shards(): lax.all_gather(shared_hidden, 'tp', axis=1, tiled=True)  19.5 us
    reduce_scatter x1, waiting for transfers between devices, shards(): lax.psum_scatter(jnp.dot(mixed_heads, out_weight, preferred_element_type=...  11.8 us
  transfers between devices with their start and end apart: 8, of which 5 were waited for; matrix products, arithmetic and copies ran while one was open for 19% of the time, Pallas kernels for 0%

profile of v1, /device:TPU:8, one launch (start us, length us, event | category | flops | bytes accessed | tf_op | source)
XLA Modules:
  0.0 500.3 jit_solution(1253674713559671481)
XLA Ops:
  13.2 4.8 reduce-window.6
  18.9 25.4 %scatter_fusion = s32[12,64]{1,0:T(8,128)S(1)} fusion(s32[12,64]{1,0:T(8,128)S(1)} %broadcast.464, s32[512]{0:T(512)S(1)} %bitcast.161, s32[512]{0:T(512)S(1)} %fusion.91), kind=kCustom, calls=%fused_computation.2 | custom fusion | bytes 10240 | tf_op jit(solution)/shard_map/scatter | solution.py:172
  44.5 4.3 gather_fusion
  48.8 3.7 copy.112
  52.5 108.1 %all_to_all.10 = bf16[12,64,2048]{2,0,1:T(8,128)(2,1)S(1)} all-to-all(bf16[12,64,2048]{2,0,1:T(8,128)(2,1)S(1)} %copy.112), channel_id=1, replica_groups=mesh['ep_0'=8,'ep_1'=4,'ep_2'=2,'tp'=4] {'ep_0','ep_1','ep_2'}, dimensions={1} | all-to-all | bytes 6291456 | tf_op jit(solution)/shard_map/all_to_all | solution.py:243
  169.9 8.6 %all-reduce.2 = f32[8]{0:T(128)S(1)} all-reduce(f32[8]{0:T(128)S(1)} %get-tuple-element.36), channel_id=4, replica_groups=mesh['ep_0'=8,'ep_1'=4,'ep_2'=2,'tp'=4] {'ep_1'}, use_global_device_ids=true, to_apply=%add.2 | all-reduce | flops 8 | bytes 64
  178.5 14.4 %all-gather.3 = f32[8,1,2]{2,1,0:T(1,128)S(1)} all-gather(f32[1,1,2]{2,1,0:T(1,128)S(1)} %get-tuple-element.28), channel_id=1, replica_groups=mesh['ep_0'=8,'ep_1'=4,'ep_2'=2,'tp'=4] {'ep_0'}, dimensions={0}, use_global_device_ids=true | all-gather | bytes 72 | tf_op jit(solution)/shard_map/all_gather | solution.py:57
  201.4 80.1 %all-gather.12.cloned.1.call-done = bf16[48,64,2048]{2,1,0:T(8,128)(2,1)} async-done(((bf16[12,64,2048]{2,1,0:T(8,128)(2,1)}), bf16[48,64,2048]{2,1,0:T(8,128)(2,1)}) %all-gather.12.cloned.1.call-update) | async-done | bytes 12582928 | tf_op jit(solution)/shard_map/all_gather | solution.py:245
  281.4 7.8 %fusion.38 = f32[48,64,256]{2,1,0:T(8,128)S(1)} fusion(bf16[48,64,2048]{2,1,0:T(8,128)(2,1)} %all-gather.12.cloned.1.call-done, bf16[1,2048,256]{2,1,0:T(8,128)(2,1)} %param.29), kind=kOutput, calls=%fused_computation.50 | convolution fusion | flops 3221225472 | bytes 16777216 | tf_op jit(solution)/shard_map/snxd,xdf->snxf/dot_general | solution.py:187
  289.2 3.4 broadcast.463
  292.6 5.4 %bitcast_dynamic-update-slice_fusion.3 = (bf16[48,64,1024]{2,1,0:T(8,128)(2,1)}, bf16[48,64,1,256]{3,1,0,2:T(8,128)(2,1)}) fusion(bf16[48,64,1024]{2,1,0:T(8,128)(2,1)} %broadcast.463, s32[]{:T(128)S(6)} %select_n.297, f32[48,64,256]{2,1,0:T(8,128)S(1)} %fusion.38, bf16[48,64,2048]{2,1,0:T(8,128)(2,1)S(1)} %copy-done.17, bf16[1,2048,256]{2,1,0:T(8,128)(2,1)S(1)} %copy-done), kind=kOutput, calls=%fused_computation.26 | convolution fusion | flops 3225944064 | bytes 19922948 | tf_op jit(solution)/shard_map/snxd,xdf->snxf/dot_general | solution.py:184
  305.2 30.3 %collective-permute-done = bf16[48,64,1,256]{3,1,0,2:T(8,128)(2,1)} collective-permute-done((bf16[48,64,1,256]{3,1,0,2:T(8,128)(2,1)}, bf16[48,64,1,256]{3,1,0,2:T(8,128)(2,1)}, u32[]{:S(2)}, u32[]{:S(2)}) %collective-permute-start) | collective-permute-done | bytes 1572896 | tf_op jit(solution)/shard_map/ppermute | solution.py:26
  340.2 12.8 %all_gather.44 = f32[4,2,128,128]{3,2,1,0:T(8,128)S(1)} all-gather(f32[1,2,128,128]{3,2,1,0:T(8,128)S(1)} %fusion.67), channel_id=1, replica_groups=mesh['ep_0'=8,'ep_1'=4,'ep_2'=2,'tp'=4] {'ep_1'}, dimensions={0}, use_global_device_ids=true | all-gather | bytes 655360 | tf_op jit(solution)/shard_map/all_gather | solution.py:57
  359.6 12.8 %collective-permute-done.2 = bf16[48,64,1,256]{3,1,0,2:T(8,128)(2,1)} collective-permute-done((bf16[48,64,1,256]{3,1,0,2:T(8,128)(2,1)}, bf16[48,64,1,256]{3,1,0,2:T(8,128)(2,1)}, u32[]{:S(2)}, u32[]{:S(2)}) %collective-permute-start.2) | collective-permute-done | bytes 1572896 | tf_op jit(solution)/shard_map/ppermute | solution.py:26
  375.2 6.4 %convolution_convert_fusion.1 = bf16[48,64,512]{2,1,0:T(8,128)(2,1)S(1)} fusion(bf16[48,64,1024]{2,1,0:T(8,128)(2,1)} %bitcast_dynamic-update-slice_fusion, bf16[1,1024,512]{2,1,0:T(8,128)(2,1)S(1)} %copy-done.21), kind=kOutput, calls=%fused_computation.12 | convolution fusion | flops 3222798336 | bytes 10485760 | tf_op jit(solution)/shard_map/snxf,xfe->snxe/dot_general | solution.py:255
  381.6 3.4 copy.114
  385.1 10.8 %all-to-all-start.1 = ((bf16[48,64,512]{2,0,1:T(8,128)(2,1)}), bf16[48,64,512]{2,0,1:T(8,128)(2,1)}, u32[]{:S(2)}, u32[]{:S(2)}) async-start(bf16[48,64,512]{2,0,1:T(8,128)(2,1)} %copy.114), calls=%async_computation.2 | async-start | bytes 6291456 | tf_op jit(solution)/shard_map/all_to_all | solution.py:259
  414.3 19.5 %all_gather.47 = bf16[512,512]{1,0:T(8,128)(2,1)} all-gather(bf16[512,128]{1,0:T(8,128)(2,1)S(1)} %fusion.28), channel_id=1, replica_groups=mesh['ep_0'=8,'ep_1'=4,'ep_2'=2,'tp'=4] {'tp'}, dimensions={1}, use_global_device_ids=true | all-gather | bytes 655360 | tf_op jit(solution)/shard_map/all_gather | solution.py:253
  433.7 11.8 %reduce-scatter.2.cloned.1.call-done = bf16[128,2048]{1,0:T(8,128)(2,1)} async-done(((bf16[512,2048]{1,0:T(8,128)(2,1)}), bf16[128,2048]{1,0:T(8,128)(2,1)}) %reduce-scatter.2.cloned.1.call-update) | async-done | bytes 524304 | tf_op jit(solution)/shard_map/reduce_scatter | solution.py:225
  447.6 21.8 %all-to-all-done.1 = bf16[48,64,512]{2,0,1:T(8,128)(2,1)} async-done(((bf16[48,64,512]{2,0,1:T(8,128)(2,1)}), bf16[48,64,512]{2,0,1:T(8,128)(2,1)}, u32[]{:S(2)}, u32[]{:S(2)}) %all-to-all-start.1) | async-done | bytes 3145760 | tf_op jit(solution)/shard_map/all_to_all | solution.py:259
  469.5 3.6 copy.115
  473.1 9.2 %gather_fusion.1 = bf16[2048,512]{1,0:T(8,128)(2,1)} fusion(bf16[3072,512]{1,0:T(8,128)(2,1)S(1)} %bitcast.160, s32[2048]{0:T(1024)S(1)} %broadcast_clamp_fusion), kind=kCustom, calls=%fused_computation.1 | custom fusion | bytes 4202496 | tf_op jit(solution)/shard_map/gather | solution.py:261
  482.3 4.8 reshape.490
  487.2 4.9 multiply_reduce_fusion
  (151 shorter events, 66.3 us)
Async XLA Ops:
  7.2 285.4 %copy-start = (bf16[1,2048,256]{2,1,0:T(8,128)(2,1)S(1)}, bf16[1,2048,256]{2,1,0:T(8,128)(2,1)}, u32[]{:S(2)}) copy-start(bf16[1,2048,256]{2,1,0:T(8,128)(2,1)} %param.28) | copy-start | bytes 3145732
  7.2 5.3 %copy-start.8 = (s32[512,4]{0,1:T(4,128)S(1)}, s32[512,4]{0,1:T(4,128)}, u32[]{:S(2)}) copy-start(s32[512,4]{0,1:T(4,128)} %param.26) | copy-start | bytes 24580
  7.2 188.7 %all-gather.8.cloned.1.call-start = ((), (), s32[]{:S(2)}) async-start(), calls=%async_computation.3 | async-start | bytes 5242880 | tf_op jit(solution)/shard_map/all_gather | solution.py:73
  12.4 269.0 %all-gather.12.cloned.1.call-start = ((), (), s32[]{:S(2)}) async-start(), calls=%async_computation.6 | async-start | bytes 15728640 | tf_op jit(solution)/shard_map/all_gather | solution.py:245
  164.0 4.5 copy-start.24
  164.0 31.9 %copy-start.19 = (bf16[2048,256]{1,0:T(8,128)(2,1)S(1)}, bf16[2048,256]{1,0:T(8,128)(2,1)}, u32[]{:S(2)}) copy-start(bf16[2048,256]{1,0:T(8,128)(2,1)} %param.21) | copy-start | bytes 3145732
  164.0 235.9 %all-gather.10.cloned.1.call-start = ((), (), s32[]{:S(2)}) async-start(), calls=%async_computation.4 | async-start | bytes 1179648 | tf_op jit(solution)/shard_map/all_gather | solution.py:57
  281.4 11.2 %copy-start.17 = (bf16[48,64,2048]{2,1,0:T(8,128)(2,1)S(1)}, bf16[48,64,2048]{2,1,0:T(8,128)(2,1)}, u32[]{:S(2)}) copy-start(bf16[48,64,2048]{2,1,0:T(8,128)(2,1)} %all-gather.12.cloned.1.call-done) | copy-start | bytes 37748740
  292.6 8.1 %copy-start.20 = (bf16[2048,256]{1,0:T(8,128)(2,1)S(1)}, bf16[2048,256]{1,0:T(8,128)(2,1)}, u32[]{:S(2)}) copy-start(bf16[2048,256]{1,0:T(8,128)(2,1)} %param.23) | copy-start | bytes 3145732
  298.0 37.5 %collective-permute-start = (bf16[48,64,1,256]{3,1,0,2:T(8,128)(2,1)}, bf16[48,64,1,256]{3,1,0,2:T(8,128)(2,1)}, u32[]{:S(2)}, u32[]{:S(2)}) collective-permute-start(bf16[48,64,1,256]{3,1,0,2:T(8,128)(2,1)} %get-tuple-element.44), channel_id=1, source_target_pairs={{0,1},{1,2},{2,3},{3,0},{4,5},{5,6},{6,7},{7,4},{8,9},{9,10},{10,1... | collective-permute-start | bytes 4718600 | tf_op jit(solution)/shard_map/ppermute | solution.py:26
  302.0 54.7 %collective-permute-start.1 = (bf16[48,64,1,256]{3,1,0,2:T(8,128)(2,1)}, bf16[48,64,1,256]{3,1,0,2:T(8,128)(2,1)}, u32[]{:S(2)}, u32[]{:S(2)}) collective-permute-start(bf16[48,64,1,256]{3,1,0,2:T(8,128)(2,1)} %get-tuple-element.44), channel_id=1, source_target_pairs={{0,3},{1,0},{2,1},{3,2},{4,7},{5,4},{6,5},{7,6},{8,11},{9,8},{10,9... | collective-permute-start | bytes 4718600 | tf_op jit(solution)/shard_map/ppermute | solution.py:35
  304.1 35.3 %copy-start.2 = (bf16[8,64,2,128]{3,2,1,0:T(2,128)(2,1)}, bf16[8,64,2,128]{3,2,1,0:T(2,128)(2,1)S(1)}, u32[]{:S(2)}) copy-start(bf16[8,64,2,128]{3,2,1,0:T(2,128)(2,1)S(1)} %reshape_reshape.3) | copy-start | bytes 786436
  335.5 36.8 %collective-permute-start.2 = (bf16[48,64,1,256]{3,1,0,2:T(8,128)(2,1)}, bf16[48,64,1,256]{3,1,0,2:T(8,128)(2,1)}, u32[]{:S(2)}, u32[]{:S(2)}) collective-permute-start(bf16[48,64,1,256]{3,1,0,2:T(8,128)(2,1)} %collective-permute-done), channel_id=1, source_target_pairs={{0,1},{1,2},{2,3},{3,0},{4,5},{5,6},{6,7},{7,4},{8,9},{9,10},{10,1... | collective-permute-start | bytes 4718600 | tf_op jit(solution)/shard_map/ppermute | solution.py:26
  356.7 18.5 %copy-start.21 = (bf16[1,1024,512]{2,1,0:T(8,128)(2,1)S(1)}, bf16[1,1024,512]{2,1,0:T(8,128)(2,1)}, u32[]{:S(2)}) copy-start(bf16[1,1024,512]{2,1,0:T(8,128)(2,1)} %param.30) | copy-start | bytes 3145732
  385.1 84.4 %all-to-all-start.1 = ((bf16[48,64,512]{2,0,1:T(8,128)(2,1)}), bf16[48,64,512]{2,0,1:T(8,128)(2,1)}, u32[]{:S(2)}, u32[]{:S(2)}) async-start(bf16[48,64,512]{2,0,1:T(8,128)(2,1)} %copy.114), calls=%async_computation.2 | async-start | bytes 6291456 | tf_op jit(solution)/shard_map/all_to_all | solution.py:259
  395.8 4.0 copy-start.10
  395.8 4.0 copy-start.11
  395.9 4.0 copy-start.12
  395.9 4.0 copy-start.13
  395.9 49.6 %reduce-scatter.2.cloned.1.call-start = ((), (), s32[]{:S(2)}) async-start(), calls=%async_computation.5 | async-start | bytes 2621440 | tf_op jit(solution)/shard_map/reduce_scatter | solution.py:225
  405.8 3.8 copy-start.22
  482.3 11.1 %copy-start.1 = (bf16[1,2048,256]{2,1,0:T(8,128)(2,1)S(1)}, bf16[1,2048,256]{2,1,0:T(8,128)(2,1)}, u32[]{:S(2)}) copy-start(bf16[1,2048,256]{2,1,0:T(8,128)(2,1)} %param.28) | copy-start | bytes 3145732
  487.2 4.9 copy-start.4
  487.2 4.9 copy-start.7
  (10 other events, 20.4 us)
Sparse Core Ops, SparseCore 0:
  12.5 53.5 all-gather.7
  164.1 117.2 all-gather.11
  354.0 39.9 all-gather.9
  409.4 36.1 reduce-scatter.1
